TPU v7x, 32 devices: a whole 2x2x4 slice. The times are simulated.
32 devices in a mesh: ep: 8 (over z, x), tp: 4 (over y, core).
Axes of the slice: x: 2, y: 2, z: 4, core: 2. Of those that a mesh axis runs over, the one named last changes fastest.
Arguments:
- hidden_in: bfloat16 [128, 1024], P('ep'), may hold values from -6 to 6
- attn_gain: float32 [1024], replicated, may hold values from 0.1 to 1.9
- w_qdown: bfloat16 [1024, 256], replicated, may hold values from -0.1875 to 0.1875
- q_gain: float32 [256], replicated, may hold values from 0.1 to 1.9
- w_qnope: bfloat16 [256, 512], replicated, may hold values from -0.375 to 0.375
- w_qrope: bfloat16 [256, 256], replicated, may hold values from -0.375 to 0.375
- w_kvdown: bfloat16 [1024, 128], replicated, may hold values from -0.1875 to 0.1875
- kv_gain: float32 [128], replicated, may hold values from 0.1 to 1.9
- w_krope: bfloat16 [1024, 32], replicated, may hold values from -0.1875 to 0.1875
- w_ukey: bfloat16 [128, 512], replicated, may hold values from -0.75 to 0.75
- w_uvalue: bfloat16 [128, 512], replicated, may hold values from -0.5 to 0.5
- w_out: bfloat16 [512, 1024], P('tp'), may hold values from -0.25 to 0.25
- cache_latent: bfloat16 [128, 1024, 128], P(('ep', 'tp')), may hold values from -6 to 6
- cache_rope: bfloat16 [128, 32, 1024], P(('ep', 'tp')), may hold values from -900 to 900
- lengths: int32 [128], P(('ep', 'tp')), may hold values from 1 to 1024, as said below
- ffn_gain: float32 [1024], replicated, may hold values from 0.1 to 1.9
- routes: int32 [128, 2], P('ep'), may hold values from 0 to 3, all different within a row; in each aligned block of 16 rows (0 to 15, 16 to 31, ...) at most 16 rows name the same one
- route_weights: float32 [128, 2], P('ep'), may hold values from 0.25 to 1
- w_gate: bfloat16 [8, 1024, 1792], P('ep', None, 'tp'), may hold values from -0.1875 to 0.1875
- w_up: bfloat16 [8, 1024, 1792], P('ep', None, 'tp'), may hold values from -0.1875 to 0.1875
- w_down: bfloat16 [8, 1792, 1024], P('ep', 'tp'), may hold values from -0.09375 to 0.09375
Outputs:
- next_hidden: bfloat16 [128, 1024], P('ep', 'tp')
Inputs may be any that keep to these rules, and one draw needn't show every extreme that they name: `lengths`: each sequence has 1 to 1024 valid cached positions; in every aligned block of 16 sequences one has all 1024. `routes`: each row names two different experts. In the aligned blocks of 16 rows no expert is named by more than 16 rows, and in some block one expert is named by exactly 16.
All inputs are finite; a program needn't handle non-finite values.
Results may differ from a plain program's by a relative error of at most 0.014.
The roundings to bfloat16 on the way count: a program that leaves them out, or rounds other values in their place, can miss the bound.
Values may be sent and summed in bfloat16 or wider, within the bound.
A program may use at most 64 MiB of HBM per device.

v0:
```python
import jax
import jax.numpy as jnp
from jax import lax
from jax.sharding import PartitionSpec as P

HEADS = 8
NOPE = 64
ROPE = 32
VDIM = 64
KVLORA = 128
eps = 1e-06
rope_base = 10000.0


def rms_scale(values, gain):
    return values * lax.rsqrt(jnp.mean(values * values, axis=-1, keepdims=True) + eps) * gain


def rotate(values, positions):
    width = values.shape[-1]
    middle = width // 2
    inverse = jnp.power(rope_base, -jnp.arange(0, width, 2).astype(jnp.float32) / width)
    angles = positions.astype(jnp.float32)[:, None] * inverse[None, :]
    angles = jnp.concatenate([angles, angles], axis=-1)
    target = (angles.shape[0],) + (1,) * (values.ndim - 2) + (width,)
    cosine = jnp.cos(angles).reshape(target)
    sine = jnp.sin(angles).reshape(target)
    turned = jnp.concatenate([-values[..., middle:], values[..., :middle]], axis=-1)
    return values * cosine + turned * sine


def route_slots(route_table, expert_count):
    flat_ids = route_table.reshape(-1)
    onehot = (flat_ids[:, None] == jnp.arange(expert_count, dtype=jnp.int32)[None, :]).astype(
        jnp.int32
    )
    before = jnp.cumsum(onehot, axis=0) - onehot
    return jnp.sum(before * onehot, axis=1).reshape(route_table.shape)


def unit_block(arrived, w_gate, w_up, w_down):
    gate_part = jnp.einsum("scd,df->scf", arrived, w_gate[0], preferred_element_type=jnp.float32)
    up_part = jnp.einsum("scd,df->scf", arrived, w_up[0], preferred_element_type=jnp.float32)
    inner = (jax.nn.silu(gate_part) * up_part).astype(jnp.bfloat16)
    block_term = jnp.einsum("scf,fd->scd", inner, w_down[0], preferred_element_type=jnp.float32)
    summed = lax.psum_scatter(
        block_term.astype(jnp.bfloat16), "tp", scatter_dimension=2, tiled=True
    )
    return lax.all_to_all(summed, "ep", split_axis=0, concat_axis=0, tiled=True)


def per_device(
    hidden_in,
    attn_gain,
    w_qdown,
    q_gain,
    w_qnope,
    w_qrope,
    w_kvdown,
    kv_gain,
    w_krope,
    w_ukey,
    w_uvalue,
    w_out,
    cache_latent,
    cache_rope,
    lengths,
    ffn_gain,
    routes,
    route_weights,
    w_gate,
    w_up,
    w_down,
):
    group_rows, width = hidden_in.shape
    own_count = lengths.shape[0]
    tp_rank = lax.axis_index("tp")
    score_scale = (NOPE + ROPE) ** (-0.5)
    own_rows = lax.dynamic_slice_in_dim(hidden_in, tp_rank * own_count, own_count, 0).astype(
        jnp.float32
    )
    normed = rms_scale(own_rows, attn_gain).astype(jnp.bfloat16)
    q_small = rms_scale(
        jnp.dot(normed, w_qdown, preferred_element_type=jnp.float32), q_gain
    ).astype(jnp.bfloat16)
    q_plain = (
        jnp.dot(q_small, w_qnope, preferred_element_type=jnp.float32)
        .astype(jnp.bfloat16)
        .reshape(own_count, HEADS, NOPE)
    )
    q_turned = rotate(
        jnp.dot(q_small, w_qrope, preferred_element_type=jnp.float32).reshape(
            own_count, HEADS, ROPE
        ),
        lengths,
    ).astype(jnp.bfloat16)
    q_latent = jnp.einsum(
        "shn,chn->shc",
        q_plain,
        w_ukey.reshape(KVLORA, HEADS, NOPE),
        preferred_element_type=jnp.float32,
    ).astype(jnp.bfloat16)
    new_latent = rms_scale(
        jnp.dot(normed, w_kvdown, preferred_element_type=jnp.float32), kv_gain
    ).astype(jnp.bfloat16)
    new_rope = rotate(jnp.dot(normed, w_krope, preferred_element_type=jnp.float32), lengths).astype(
        jnp.bfloat16
    )
    past_scores = (
        jnp.einsum("shc,spc->shp", q_latent, cache_latent, preferred_element_type=jnp.float32)
        + jnp.einsum("shr,srp->shp", q_turned, cache_rope, preferred_element_type=jnp.float32)
    ) * score_scale
    in_range = jnp.arange(cache_latent.shape[1])[None, None, :] < lengths[:, None, None]
    past_scores = jnp.where(in_range, past_scores, -1e30)
    fresh_score = (
        jnp.einsum("shc,sc->sh", q_latent, new_latent, preferred_element_type=jnp.float32)
        + jnp.einsum("shr,sr->sh", q_turned, new_rope, preferred_element_type=jnp.float32)
    ) * score_scale
    highest = jnp.maximum(jnp.max(past_scores, axis=-1), fresh_score)
    past_exp = jnp.exp(past_scores - highest[..., None])
    fresh_exp = jnp.exp(fresh_score - highest)
    divisor = jnp.sum(past_exp, axis=-1) + fresh_exp
    past_prob = (past_exp / divisor[..., None]).astype(jnp.bfloat16)
    fresh_prob = (fresh_exp / divisor).astype(jnp.bfloat16)
    latent_mix = (
        jnp.einsum("shp,spc->shc", past_prob, cache_latent, preferred_element_type=jnp.float32)
        + fresh_prob.astype(jnp.float32)[..., None] * new_latent.astype(jnp.float32)[:, None, :]
    ).astype(jnp.bfloat16)
    head_values = (
        jnp.einsum(
            "shc,chv->shv",
            latent_mix,
            w_uvalue.reshape(KVLORA, HEADS, VDIM),
            preferred_element_type=jnp.float32,
        )
        .astype(jnp.bfloat16)
        .reshape(own_count, HEADS * VDIM)
    )
    by_heads = lax.all_to_all(head_values, "tp", split_axis=1, concat_axis=0, tiled=True)
    attended = lax.psum(
        jnp.dot(by_heads, w_out, preferred_element_type=jnp.float32).astype(jnp.bfloat16), "tp"
    ).astype(jnp.float32)
    residual = hidden_in.astype(jnp.float32) + attended
    normed_two = rms_scale(residual, ffn_gain).astype(jnp.bfloat16)
    unit_count = lax.axis_size("ep")
    expert_count = unit_count // 2
    capacity = max(2, 4 * group_rows // expert_count)
    quarter = width // lax.axis_size("tp")
    slots = route_slots(routes, expert_count)
    expert_of_unit = jnp.arange(unit_count, dtype=jnp.int32) // 2
    slot_range = jnp.arange(capacity, dtype=jnp.int32)
    chosen = (routes[None, None, :, :] == expert_of_unit[:, None, None, None]) & (
        slots[None, None, :, :] == slot_range[None, :, None, None]
    )
    chooser = jnp.sum(chosen.astype(jnp.int32), axis=-1).astype(jnp.bfloat16)
    outgoing = jnp.einsum(
        "ucr,rd->ucd", chooser, normed_two, preferred_element_type=jnp.float32
    ).astype(jnp.bfloat16)
    returned = unit_block(
        lax.all_to_all(outgoing, "ep", split_axis=0, concat_axis=0, tiled=True),
        w_gate,
        w_up,
        w_down,
    )
    stacked = returned.reshape(unit_count * capacity, quarter)
    first_row = routes * (2 * capacity) + slots
    first_half = stacked[first_row].astype(jnp.float32)
    second_half = stacked[first_row + capacity].astype(jnp.float32)
    blended = jnp.sum(route_weights[..., None] * (first_half + second_half), axis=1)
    own_columns = lax.dynamic_slice_in_dim(residual, tp_rank * quarter, quarter, 1)
    return (own_columns + blended).astype(jnp.bfloat16)


def solution(mesh):
    placed = (
        P("ep", None),
        P(),
        P(),
        P(),
        P(),
        P(),
        P(),
        P(),
        P(),
        P(),
        P(),
        P("tp", None),
        P(("ep", "tp"), None, None),
        P(("ep", "tp"), None, None),
        P(("ep", "tp")),
        P(),
        P("ep", None),
        P("ep", None),
        P("ep", None, "tp"),
        P("ep", None, "tp"),
        P("ep", "tp", None),
    )
    return jax.shard_map(
        per_device, mesh=mesh, in_specs=placed, out_specs=P("ep", "tp"), check_vma=False
    )
```

profile of v0, /device:TPU:0, one launch (start us, length us, event | category | flops | bytes accessed | tf_op | source)
XLA Modules:
  0.0 95.3 jit_solution(16051706030308229401)
XLA Ops:
  6.5 0.8 convert_element_type.106
  7.3 0.7 iota_compare_fusion.2
  8.0 0.8 fusion.25
  8.9 1.1 %fusion.49 = f32[4,32]{1,0:T(4,128)S(1)} fusion(bf16[1024,32]{0,1:T(8,128)(2,1)} %param.29, f32[1024]{0:T(1024)} %param.22, f32[4]{0:T(128)S(1)} %add_rsqrt_fusion.3, bf16[16,1024]{1,0:T(8,128)(2,1)S(1)} %copy-done.4, s32[]{:T(128)S(6)} %select_n.25), kind=kOutput, calls=%fused_computation.101 | convolution fusion | flops 278528 | bytes 78852 | tf_op jit(solution)/shard_map/dot_general | solution.py:106
  10.0 1.4 %multiply_reduce_fusion.2 = (f32[4]{0:T(128)S(1)}, f32[4,256]{1,0:T(4,128)S(1)}) fusion(bf16[1024,256]{1,0:T(8,128)(2,1)} %param.23, f32[1024]{0:T(1024)S(1)} %copy-done.8, f32[4]{0:T(128)S(1)} %add_rsqrt_fusion.3, bf16[16,1024]{1,0:T(8,128)(2,1)S(1)} %copy-done.4, s32[]{:T(128)S(6)} %select_n.25), kind=kOutput, calls=%fused_computation.66 | convolution fusion | flops 2115580 | bytes 541204 | tf_op jit(solution)/shard_map/dot_general | solution.py:84
  11.4 0.7 copy-done.16
  12.4 0.2 convolution_convert_fusion.5
  12.7 0.6 copy-done.5
  13.9 0.4 copy-done.14
  14.3 0.3 multiply_reduce_fusion.3
  14.8 0.7 copy-done.11
  15.7 0.5 fusion.56
  16.1 0.2 fusion.17
  16.3 0.7 copy-done.6
  17.2 0.3 fusion.3
  17.5 0.2 fusion.5
  17.8 0.6 copy.74
  18.4 4.3 %all-to-all-start = ((bf16[4,4,128]{2,0,1:T(4,128)(2,1)}), bf16[4,4,128]{2,0,1:T(4,128)(2,1)S(1)}, u32[]{:S(2)}, u32[]{:S(2)}) async-start(bf16[4,4,128]{2,0,1:T(4,128)(2,1)} %copy.74), calls=%async_computation | async-start | bytes 8192 | tf_op jit(solution)/shard_map/all_to_all | solution.py:139
  23.0 0.2 select_reduce_fusion
  23.5 3.0 %all-to-all-done = bf16[4,4,128]{2,0,1:T(4,128)(2,1)S(1)} async-done(((bf16[4,4,128]{2,0,1:T(4,128)(2,1)}), bf16[4,4,128]{2,0,1:T(4,128)(2,1)S(1)}, u32[]{:S(2)}, u32[]{:S(2)}) %all-to-all-start) | async-done | bytes 4128 | tf_op jit(solution)/shard_map/all_to_all | solution.py:139
  26.6 10.3 %psum.7 = bf16[16,1024]{1,0:T(8,128)(2,1)S(1)} all-reduce(bf16[16,1024]{1,0:T(8,128)(2,1)S(1)} %convolution_convert_fusion.2), channel_id=1, replica_groups=mesh['ep'=8,'tp'=4] {'tp'}, use_global_device_ids=true, to_apply=%region_5.6 | all-reduce | flops 16384 | bytes 65536 | tf_op jit(solution)/shard_map/psum | solution.py:140
  37.0 0.3 convolution_convert_fusion
  37.3 15.4 %all_to_all.29 = bf16[8,16,1024]{2,1,0:T(8,128)(2,1)S(1)} all-to-all(bf16[8,16,1024]{2,1,0:T(8,128)(2,1)S(1)} %convolution_convert_fusion), channel_id=1, replica_groups=mesh['ep'=8,'tp'=4] {'ep'}, dimensions={0} | all-to-all | bytes 524288 | tf_op jit(solution)/shard_map/all_to_all | solution.py:160
  52.7 0.4 fusion.9
  53.1 2.6 %convolution_convert_fusion.1 = bf16[8,16,1024]{2,1,0:T(8,128)(2,1)} fusion(bf16[8,16,1024]{2,1,0:T(8,128)(2,1)S(1)} %all_to_all.29, bf16[1,448,1024]{2,1,0:T(8,128)(2,1)S(1)} %copy-done.12, bf16[1,1024,448]{1,2,0:T(8,128)(2,1)} %param.40, f32[8,16,448]{2,1,0:T(8,128)S(1)} %fusion.9), kind=kOutput, calls=%fused_computation.3 | convolution fusion | flops 235356160 | bytes 2588672 | tf_op jit(solution)/shard_map/scf,fd->scd/dot_general | solution.py:45
  55.9 18.1 %reduce-scatter.2.cloned.1.call-done = bf16[8,16,256]{2,1,0:T(8,128)(2,1)} async-done(((bf16[8,16,1024]{2,1,0:T(8,128)(2,1)}), bf16[8,16,256]{2,1,0:T(8,128)(2,1)}) %reduce-scatter.2.cloned.1.call-update) | async-done | bytes 65552 | tf_op jit(solution)/shard_map/reduce_scatter | solution.py:46
  74.0 5.5 %all-to-all-start.2 = ((bf16[8,16,256]{2,1,0:T(8,128)(2,1)}), bf16[8,16,256]{2,1,0:T(8,128)(2,1)S(1)}, u32[]{:S(2)}, u32[]{:S(2)}) async-start(bf16[8,16,256]{2,1,0:T(8,128)(2,1)} %reduce-scatter.2.cloned.1.call-done), calls=%async_computation.3 | async-start | bytes 131072 | tf_op jit(solution)/shard_map/all_to_all | solution.py:49
  79.7 0.6 copy-done.10
  80.4 6.0 %all-to-all-done.2 = bf16[8,16,256]{2,1,0:T(8,128)(2,1)S(1)} async-done(((bf16[8,16,256]{2,1,0:T(8,128)(2,1)}), bf16[8,16,256]{2,1,0:T(8,128)(2,1)S(1)}, u32[]{:S(2)}, u32[]{:S(2)}) %all-to-all-start.2) | async-done | bytes 65568 | tf_op jit(solution)/shard_map/all_to_all | solution.py:49
  86.4 0.6 gather_fusion
  87.1 0.6 gather_fusion.1
  87.8 0.6 add_convert_fusion
  (76 shorter events, 3.2 us)
Async XLA Ops:
  6.5 9.1 %copy-start = (bf16[4,1024,128]{2,1,0:T(8,128)(2,1)S(1)}, bf16[4,1024,128]{2,1,0:T(8,128)(2,1)}, u32[]{:S(2)}) copy-start(bf16[4,1024,128]{2,1,0:T(8,128)(2,1)} %param.33) | copy-start | bytes 3145732
  6.5 2.3 %copy-start.4 = (bf16[16,1024]{1,0:T(8,128)(2,1)S(1)}, bf16[16,1024]{1,0:T(8,128)(2,1)}, u32[]{:S(2)}) copy-start(bf16[16,1024]{1,0:T(8,128)(2,1)} %param.21) | copy-start | bytes 98308
  8.9 1.1 %copy-start.8 = (f32[1024]{0:T(1024)S(1)}, f32[1024]{0:T(1024)}, u32[]{:S(2)}) copy-start(f32[1024]{0:T(1024)} %param.22) | copy-start | bytes 12292
  10.0 1.5 %copy-start.15 = (bf16[256,256]{1,0:T(8,128)(2,1)S(1)}, bf16[256,256]{1,0:T(8,128)(2,1)}, u32[]{:S(2)}) copy-start(bf16[256,256]{1,0:T(8,128)(2,1)} %param.26) | copy-start | bytes 393220
  10.0 2.5 %copy-start.13 = (bf16[256,512]{1,0:T(8,128)(2,1)S(1)}, bf16[256,512]{1,0:T(8,128)(2,1)}, u32[]{:S(2)}) copy-start(bf16[256,512]{1,0:T(8,128)(2,1)} %param.25) | copy-start | bytes 786436
  11.4 0.7 copy-start.16
  12.3 0.9 copy-start.5
  12.4 1.3 %copy-start.3 = (bf16[4,32,1024]{2,1,0:T(8,128)(2,1)S(1)}, bf16[4,32,1024]{2,1,0:T(8,128)(2,1)}, u32[]{:S(2)}) copy-start(bf16[4,32,1024]{2,1,0:T(8,128)(2,1)} %param.34) | copy-start | bytes 786436
  13.4 1.0 %copy-start.14 = (bf16[1024,128]{1,0:T(8,128)(2,1)S(1)}, bf16[1024,128]{1,0:T(8,128)(2,1)}, u32[]{:S(2)}) copy-start(bf16[1024,128]{1,0:T(8,128)(2,1)} %param.27) | copy-start | bytes 786436
  14.8 0.7 copy-start.11
  16.1 0.9 copy-start.6
  17.2 5.5 %copy-start.7 = (s32[16,2]{0,1:T(2,128)S(1)}, s32[16,2]{0,1:T(2,128)}, u32[]{:S(2)}) copy-start(s32[16,2]{0,1:T(2,128)} %param.37) | copy-start | bytes 388
  17.2 9.3 %copy-start.2 = (bf16[128,1024]{1,0:T(8,128)(2,1)S(1)}, bf16[128,1024]{1,0:T(8,128)(2,1)}, u32[]{:S(2)}) copy-start(bf16[128,1024]{1,0:T(8,128)(2,1)} %param.32) | copy-start | bytes 786436
  17.2 19.8 %copy-start.9 = (f32[1024]{0:T(1024)S(1)}, f32[1024]{0:T(1024)}, u32[]{:S(2)}) copy-start(f32[1024]{0:T(1024)} %param.36) | copy-start | bytes 12292
  17.5 35.2 %copy-start.1 = (bf16[1,1024,448]{1,2,0:T(8,128)(2,1)S(1)}, bf16[1,1024,448]{1,2,0:T(8,128)(2,1)}, u32[]{:S(2)}) copy-start(bf16[1,1024,448]{1,2,0:T(8,128)(2,1)} %param.39) | copy-start | bytes 2752516
  18.4 8.1 %all-to-all-start = ((bf16[4,4,128]{2,0,1:T(4,128)(2,1)}), bf16[4,4,128]{2,0,1:T(4,128)(2,1)S(1)}, u32[]{:S(2)}, u32[]{:S(2)}) async-start(bf16[4,4,128]{2,0,1:T(4,128)(2,1)} %copy.74), calls=%async_computation | async-start | bytes 8192 | tf_op jit(solution)/shard_map/all_to_all | solution.py:139
  22.7 51.3 %reduce-scatter.2.cloned.1.call-start = ((), (), s32[]{:S(2)}) async-start(), calls=%async_computation.4 | async-start | bytes 327680 | tf_op jit(solution)/shard_map/reduce_scatter | solution.py:46
  37.3 15.8 %copy-start.12 = (bf16[1,448,1024]{2,1,0:T(8,128)(2,1)S(1)}, bf16[1,448,1024]{2,1,0:T(8,128)(2,1)}, u32[]{:S(2)}) copy-start(bf16[1,448,1024]{2,1,0:T(8,128)(2,1)} %param.41) | copy-start | bytes 2752516
  74.0 12.4 %all-to-all-start.2 = ((bf16[8,16,256]{2,1,0:T(8,128)(2,1)}), bf16[8,16,256]{2,1,0:T(8,128)(2,1)S(1)}, u32[]{:S(2)}, u32[]{:S(2)}) async-start(bf16[8,16,256]{2,1,0:T(8,128)(2,1)} %reduce-scatter.2.cloned.1.call-done), calls=%async_computation.3 | async-start | bytes 131072 | tf_op jit(solution)/shard_map/all_to_all | solution.py:49
  79.6 0.7 copy-start.10
Sparse Core Ops, SparseCore 0:
  55.9 18.0 reduce-scatter.1
where the time goes:
time: 95.9 us; the launch traced here: 95.3 us
  waiting for transfers between devices  27.1 us (28%)
  blocking collectives  25.6 us (27%)
  between operations  13.6 us (14%)
  starting transfers between devices  9.79 us (10%)
  matrix products  8.07 us (8%)
  local copies, waits for them, and re-layouts  6.79 us (7%)
  other arithmetic  4.28 us (4%)
    reduce_scatter x1, waiting for transfers between devices, unit_block(): lax.psum_scatter(block_term.astype(jnp.bfloat16), 'tp', scatter_dimension...  18.1 us
    all_to_all x1, blocking collectives, per_device(): lax.all_to_all(outgoing, 'ep', split_axis=0, concat_axis=0, tiled=True)  15.4 us
    psum x1, blocking collectives, per_device(): lax.psum(jnp.dot(by_heads, w_out, preferred_element_type=jnp.float32).ast...  10.3 us
    all_to_all x1, waiting for transfers between devices, unit_block(): return lax.all_to_all(summed, 'ep', split_axis=0, concat_axis=0, tiled=True)  6.04 us
    all_to_all x1, starting transfers between devices, unit_block(): return lax.all_to_all(summed, 'ep', split_axis=0, concat_axis=0, tiled=True)  5.52 us
    all_to_all x1, starting transfers between devices, per_device(): lax.all_to_all(head_values, 'tp', split_axis=1, concat_axis=0, tiled=True)  4.26 us
    unnamed x38, local copies, waits for them, and re-layouts  4.04 us
    all_to_all x1, waiting for transfers between devices, per_device(): lax.all_to_all(head_values, 'tp', split_axis=1, concat_axis=0, tiled=True)  2.99 us
  transfers between devices with their start and end apart: 3, of which 3 were waited for; matrix products, arithmetic and copies ran while one was open for 1% of the time, Pallas kernels for 0%

commit v1 on v0

--- a/solution.py
+++ b/solution.py
@@ -136,7 +136,15 @@
         .astype(jnp.bfloat16)
         .reshape(own_count, HEADS * VDIM)
     )
-    by_heads = lax.all_to_all(head_values, "tp", split_axis=1, concat_axis=0, tiled=True)
+    by_heads = jnp.concatenate(
+        jax.lax.all_to_all(
+            jnp.stack(jnp.split(head_values, jax.lax.psum(1, "tp"), 1), 0),
+            concat_axis=0,
+            split_axis=0,
+            axis_name="tp",
+        ),
+        0,
+    )
     attended = lax.psum(
         jnp.dot(by_heads, w_out, preferred_element_type=jnp.float32).astype(jnp.bfloat16), "tp"
     ).astype(jnp.float32)

time: 95.9 us -> 95.9 us (level)
  no operation moved by 1% of the time
where the time goes in v1:
time: 95.9 us; the launch traced here: 95.3 us
  waiting for transfers between devices  27.1 us (28%)
  blocking collectives  25.6 us (27%)
  between operations  13.6 us (14%)
  starting transfers between devices  9.79 us (10%)
  matrix products  8.08 us (8%)
  local copies, waits for them, and re-layouts  6.18 us (6%)
  other arithmetic  4.9 us (5%)
    reduce_scatter x1, waiting for transfers between devices, unit_block(): lax.psum_scatter(block_term.astype(jnp.bfloat16), 'tp', scatter_dimension...  18.1 us
    all_to_all x1, blocking collectives, per_device(): lax.all_to_all(outgoing, 'ep', split_axis=0, concat_axis=0, tiled=True)  15.3 us
    psum x1, blocking collectives, per_device(): lax.psum(jnp.dot(by_heads, w_out, preferred_element_type=jnp.float32).ast...  10.3 us
    all_to_all x1, waiting for transfers between devices, unit_block(): return lax.all_to_all(summed, 'ep', split_axis=0, concat_axis=0, tiled=True)  6.04 us
    all_to_all x1, starting transfers between devices, unit_block(): return lax.all_to_all(summed, 'ep', split_axis=0, concat_axis=0, tiled=True)  5.52 us
    all_to_all x1, starting transfers between devices, per_device(): jax.lax.all_to_all(jnp.stack(jnp.split(head_values, jax.lax.psum(1, 'tp')...  4.26 us
    unnamed x38, local copies, waits for them, and re-layouts  4.04 us
    all_to_all x1, waiting for transfers between devices, per_device(): jax.lax.all_to_all(jnp.stack(jnp.split(head_values, jax.lax.psum(1, 'tp')...  2.99 us
  transfers between devices with their start and end apart: 3, of which 3 were waited for; matrix products, arithmetic and copies ran while one was open for 1% of the time, Pallas kernels for 0%

profile of v1, /device:TPU:0, one launch (start us, length us, event | category | flops | bytes accessed | tf_op | source)
XLA Modules:
  0.0 95.3 jit_solution(2506243411484095402)
XLA Ops:
  6.5 0.8 convert_element_type.106
  7.3 0.7 iota_compare_fusion.2
  8.0 0.8 fusion.25
  8.9 1.1 %fusion.49 = f32[4,32]{1,0:T(4,128)S(1)} fusion(bf16[1024,32]{0,1:T(8,128)(2,1)} %param.29, f32[1024]{0:T(1024)} %param.22, f32[4]{0:T(128)S(1)} %add_rsqrt_fusion.3, bf16[16,1024]{1,0:T(8,128)(2,1)S(1)} %copy-done.4, s32[]{:T(128)S(6)} %select_n.25), kind=kOutput, calls=%fused_computation.106 | convolution fusion | flops 278528 | bytes 78852 | tf_op jit(solution)/shard_map/dot_general | solution.py:106
  10.0 1.4 %multiply_reduce_fusion.2 = (f32[4]{0:T(128)S(1)}, f32[4,256]{1,0:T(4,128)S(1)}) fusion(bf16[1024,256]{1,0:T(8,128)(2,1)} %param.23, f32[1024]{0:T(1024)S(1)} %copy-done.8, f32[4]{0:T(128)S(1)} %add_rsqrt_fusion.3, bf16[16,1024]{1,0:T(8,128)(2,1)S(1)} %copy-done.4, s32[]{:T(128)S(6)} %select_n.25), kind=kOutput, calls=%fused_computation.67 | convolution fusion | flops 2115580 | bytes 541204 | tf_op jit(solution)/shard_map/dot_general | solution.py:84
  11.4 0.7 copy-done.16
  12.4 0.2 convolution_convert_fusion.5
  12.7 0.6 copy-done.5
  13.9 0.4 copy-done.14
  14.3 0.3 multiply_reduce_fusion.3
  14.8 0.7 copy-done.11
  15.7 0.5 fusion.56
  16.1 0.2 fusion.17
  16.3 0.7 copy-done.6
  17.2 0.3 fusion.3
  17.5 0.2 fusion.5
  17.8 0.6 pad_maximum_fusion
  18.4 4.3 %all-to-all-start = ((bf16[4,4,128]{2,1,0:T(4,128)(2,1)}), bf16[4,4,128]{2,1,0:T(4,128)(2,1)S(1)}, u32[]{:S(2)}, u32[]{:S(2)}) async-start(bf16[4,4,128]{2,1,0:T(4,128)(2,1)} %pad_maximum_fusion), calls=%async_computation | async-start | bytes 8192 | tf_op jit(solution)/shard_map/all_to_all | solution.py:140
  23.0 0.2 select_reduce_fusion
  23.5 3.0 %all-to-all-done = bf16[4,4,128]{2,1,0:T(4,128)(2,1)S(1)} async-done(((bf16[4,4,128]{2,1,0:T(4,128)(2,1)}), bf16[4,4,128]{2,1,0:T(4,128)(2,1)S(1)}, u32[]{:S(2)}, u32[]{:S(2)}) %all-to-all-start) | async-done | bytes 4128 | tf_op jit(solution)/shard_map/all_to_all | solution.py:140
  26.6 10.3 %psum.7 = bf16[16,1024]{1,0:T(8,128)(2,1)S(1)} all-reduce(bf16[16,1024]{1,0:T(8,128)(2,1)S(1)} %convolution_convert_fusion.2), channel_id=1, replica_groups=mesh['ep'=8,'tp'=4] {'tp'}, use_global_device_ids=true, to_apply=%region_5.6 | all-reduce | flops 16384 | bytes 65536 | tf_op jit(solution)/shard_map/psum | solution.py:148
  37.0 0.3 convolution_convert_fusion
  37.3 15.3 %all_to_all.15 = bf16[8,16,1024]{2,1,0:T(8,128)(2,1)S(1)} all-to-all(bf16[8,16,1024]{2,1,0:T(8,128)(2,1)S(1)} %convolution_convert_fusion), channel_id=1, replica_groups=mesh['ep'=8,'tp'=4] {'ep'}, dimensions={0} | all-to-all | bytes 524288 | tf_op jit(solution)/shard_map/all_to_all | solution.py:168
  52.7 0.4 fusion.9
  53.1 2.6 %convolution_convert_fusion.1 = bf16[8,16,1024]{2,1,0:T(8,128)(2,1)} fusion(bf16[8,16,1024]{2,1,0:T(8,128)(2,1)S(1)} %all_to_all.15, bf16[1,448,1024]{2,1,0:T(8,128)(2,1)S(1)} %copy-done.12, bf16[1,1024,448]{1,2,0:T(8,128)(2,1)} %param.40, f32[8,16,448]{2,1,0:T(8,128)S(1)} %fusion.9), kind=kOutput, calls=%fused_computation.3 | convolution fusion | flops 235356160 | bytes 2588672 | tf_op jit(solution)/shard_map/scf,fd->scd/dot_general | solution.py:45
  55.9 18.1 %reduce-scatter.2.cloned.1.call-done = bf16[8,16,256]{2,1,0:T(8,128)(2,1)} async-done(((bf16[8,16,1024]{2,1,0:T(8,128)(2,1)}), bf16[8,16,256]{2,1,0:T(8,128)(2,1)}) %reduce-scatter.2.cloned.1.call-update) | async-done | bytes 65552 | tf_op jit(solution)/shard_map/reduce_scatter | solution.py:46
  74.0 5.5 %all-to-all-start.2 = ((bf16[8,16,256]{2,1,0:T(8,128)(2,1)}), bf16[8,16,256]{2,1,0:T(8,128)(2,1)S(1)}, u32[]{:S(2)}, u32[]{:S(2)}) async-start(bf16[8,16,256]{2,1,0:T(8,128)(2,1)} %reduce-scatter.2.cloned.1.call-done), calls=%async_computation.3 | async-start | bytes 131072 | tf_op jit(solution)/shard_map/all_to_all | solution.py:49
  79.7 0.6 copy-done.10
  80.4 6.0 %all-to-all-done.2 = bf16[8,16,256]{2,1,0:T(8,128)(2,1)S(1)} async-done(((bf16[8,16,256]{2,1,0:T(8,128)(2,1)}), bf16[8,16,256]{2,1,0:T(8,128)(2,1)S(1)}, u32[]{:S(2)}, u32[]{:S(2)}) %all-to-all-start.2) | async-done | bytes 65568 | tf_op jit(solution)/shard_map/all_to_all | solution.py:49
  86.4 0.6 gather_fusion
  87.1 0.6 gather_fusion.1
  87.9 0.6 add_convert_fusion
  (77 shorter events, 3.2 us)
Async XLA Ops:
  6.5 9.1 %copy-start = (bf16[4,1024,128]{2,1,0:T(8,128)(2,1)S(1)}, bf16[4,1024,128]{2,1,0:T(8,128)(2,1)}, u32[]{:S(2)}) copy-start(bf16[4,1024,128]{2,1,0:T(8,128)(2,1)} %param.33) | copy-start | bytes 3145732
  6.5 2.3 %copy-start.4 = (bf16[16,1024]{1,0:T(8,128)(2,1)S(1)}, bf16[16,1024]{1,0:T(8,128)(2,1)}, u32[]{:S(2)}) copy-start(bf16[16,1024]{1,0:T(8,128)(2,1)} %param.21) | copy-start | bytes 98308
  8.9 1.1 %copy-start.8 = (f32[1024]{0:T(1024)S(1)}, f32[1024]{0:T(1024)}, u32[]{:S(2)}) copy-start(f32[1024]{0:T(1024)} %param.22) | copy-start | bytes 12292
  10.0 1.5 %copy-start.15 = (bf16[256,256]{1,0:T(8,128)(2,1)S(1)}, bf16[256,256]{1,0:T(8,128)(2,1)}, u32[]{:S(2)}) copy-start(bf16[256,256]{1,0:T(8,128)(2,1)} %param.26) | copy-start | bytes 393220
  10.0 2.5 %copy-start.13 = (bf16[256,512]{1,0:T(8,128)(2,1)S(1)}, bf16[256,512]{1,0:T(8,128)(2,1)}, u32[]{:S(2)}) copy-start(bf16[256,512]{1,0:T(8,128)(2,1)} %param.25) | copy-start | bytes 786436
  11.4 0.7 copy-start.16
  12.3 0.9 copy-start.5
  12.4 1.3 %copy-start.3 = (bf16[4,32,1024]{2,1,0:T(8,128)(2,1)S(1)}, bf16[4,32,1024]{2,1,0:T(8,128)(2,1)}, u32[]{:S(2)}) copy-start(bf16[4,32,1024]{2,1,0:T(8,128)(2,1)} %param.34) | copy-start | bytes 786436
  13.4 1.0 %copy-start.14 = (bf16[1024,128]{1,0:T(8,128)(2,1)S(1)}, bf16[1024,128]{1,0:T(8,128)(2,1)}, u32[]{:S(2)}) copy-start(bf16[1024,128]{1,0:T(8,128)(2,1)} %param.27) | copy-start | bytes 786436
  14.8 0.7 copy-start.11
  16.1 0.9 copy-start.6
  17.2 5.5 %copy-start.7 = (s32[16,2]{0,1:T(2,128)S(1)}, s32[16,2]{0,1:T(2,128)}, u32[]{:S(2)}) copy-start(s32[16,2]{0,1:T(2,128)} %param.37) | copy-start | bytes 388
  17.2 9.3 %copy-start.2 = (bf16[128,1024]{1,0:T(8,128)(2,1)S(1)}, bf16[128,1024]{1,0:T(8,128)(2,1)}, u32[]{:S(2)}) copy-start(bf16[128,1024]{1,0:T(8,128)(2,1)} %param.32) | copy-start | bytes 786436
  17.2 19.8 %copy-start.9 = (f32[1024]{0:T(1024)S(1)}, f32[1024]{0:T(1024)}, u32[]{:S(2)}) copy-start(f32[1024]{0:T(1024)} %param.36) | copy-start | bytes 12292
  17.5 35.2 %copy-start.1 = (bf16[1,1024,448]{1,2,0:T(8,128)(2,1)S(1)}, bf16[1,1024,448]{1,2,0:T(8,128)(2,1)}, u32[]{:S(2)}) copy-start(bf16[1,1024,448]{1,2,0:T(8,128)(2,1)} %param.39) | copy-start | bytes 2752516
  18.4 8.1 %all-to-all-start = ((bf16[4,4,128]{2,1,0:T(4,128)(2,1)}), bf16[4,4,128]{2,1,0:T(4,128)(2,1)S(1)}, u32[]{:S(2)}, u32[]{:S(2)}) async-start(bf16[4,4,128]{2,1,0:T(4,128)(2,1)} %pad_maximum_fusion), calls=%async_computation | async-start | bytes 8192 | tf_op jit(solution)/shard_map/all_to_all | solution.py:140
  22.7 51.3 %reduce-scatter.2.cloned.1.call-start = ((), (), s32[]{:S(2)}) async-start(), calls=%async_computation.4 | async-start | bytes 327680 | tf_op jit(solution)/shard_map/reduce_scatter | solution.py:46
  37.3 15.8 %copy-start.12 = (bf16[1,448,1024]{2,1,0:T(8,128)(2,1)S(1)}, bf16[1,448,1024]{2,1,0:T(8,128)(2,1)}, u32[]{:S(2)}) copy-start(bf16[1,448,1024]{2,1,0:T(8,128)(2,1)} %param.41) | copy-start | bytes 2752516
  74.0 12.4 %all-to-all-start.2 = ((bf16[8,16,256]{2,1,0:T(8,128)(2,1)}), bf16[8,16,256]{2,1,0:T(8,128)(2,1)S(1)}, u32[]{:S(2)}, u32[]{:S(2)}) async-start(bf16[8,16,256]{2,1,0:T(8,128)(2,1)} %reduce-scatter.2.cloned.1.call-done), calls=%async_computation.3 | async-start | bytes 131072 | tf_op jit(solution)/shard_map/all_to_all | solution.py:49
  79.6 0.7 copy-start.10
Sparse Core Ops, SparseCore 0:
  55.9 18.0 reduce-scatter.1
